TPU v7x, 256 devices: a 4x2x16 block of a 4x16x16 slice. The times are simulated.
256 devices in a mesh: grp: 2 (over y), sp: 32 (over z, core), tp: 4 (over x).
Axes of the slice: x: 4, y: 2, z: 16, core: 2. Of those that a mesh axis runs over, the one named last changes fastest.
The devices are a block of a 4x16x16 slice.
Arguments:
- stream: bfloat16 [16384, 4096], P(('grp', 'sp'), 'tp'), parts along dimension 0, may hold values from -6 to 6
- gain_pre: float32 [3, 4096], replicated, may hold values from 0.1 to 1.9
- w_in: bfloat16 [3, 4096, 1024], P(None, 'sp', 'tp'), may hold values from -0.09375 to 0.09375
- w_pool: bfloat16 [3, 4, 256, 256], P(None, 'tp'), may hold values from -0.375 to 0.375
- pool_scale: float32 [3, 1024], P(None, 'tp'), may hold values from 0.1 to 1.9
- w_out: bfloat16 [3, 1024, 4096], P(None, 'tp', 'sp'), may hold values from -0.5 to 0.5
- gain_post: float32 [3, 4096], replicated, may hold values from 0.1 to 1.9
Outputs:
- result: bfloat16 [16384, 4096], P(('grp', 'sp'), 'tp'), parts along dimension 0
There are 2 independent parts, one for each index of `grp`. A program takes and returns all parts, laid end to end along the dimension named above; an argument that names none is the same for every part. Nothing has to cross between parts.
All inputs are finite; a program needn't handle non-finite values.
Results may differ from a plain program's by a relative error of at most 0.02.
Values may be sent and summed in bfloat16 or wider, within the bound.
A program may use at most 64 MiB of HBM per device.

v0:
```python
import jax
import jax.numpy as jnp
from jax import lax
from jax.sharding import PartitionSpec as P

LAYERS = 3
WINDOWS = (2, 4, 8, 16)
EPS = 1e-06


def rows_first(arrays, axis, dims):
    turned = [jnp.moveaxis(a, dim, 0) for a, dim in zip(arrays, dims)]
    widths = [t[0].size for t in turned]
    both = jnp.concatenate([t.reshape(-1, w) for t, w in zip(turned, widths)], axis=1)
    result = lax.all_gather(both, axis, axis=0, tiled=True)
    tiles = jnp.split(result, [sum(widths[:k]) for k in range(1, len(widths))], axis=1)
    return tuple(
        (
            jnp.moveaxis(b.reshape(-1, *t.shape[1:]), 0, dim)
            for b, t, dim in zip(tiles, turned, dims)
        )
    )


def from_behind(block, axis, distance):
    devices = range(lax.axis_size(axis))
    route = [(i - distance, i) for i in devices if i - distance in devices]
    return lax.ppermute(block, axis, route)


def copy_for_each(array, axis):
    copies = jnp.broadcast_to(array, (lax.axis_size(axis), *array.shape))
    return lax.all_to_all(copies, axis, split_axis=0, concat_axis=0, tiled=True)


def joined_along(tiles, dim):
    tiles = jnp.moveaxis(tiles, 0, dim)
    dims = tiles.shape
    return tiles.reshape(*dims[:dim], dims[dim] * dims[dim + 1], *dims[dim + 2 :])


def gather_directly(array, axis, dim):
    tiles = copy_for_each(array, axis)
    return joined_along(tiles, dim)


def in_blocks(array, dim, size):
    before, after = (array.shape[:dim], array.shape[dim + 1 :])
    return jnp.moveaxis(array.reshape(*before, size, -1, *after), dim, 0)


def sent_and_summed(array, axis, dim):
    size = lax.axis_size(axis)
    tiles = lax.all_to_all(in_blocks(array, dim, size), axis, 0, 0, tiled=True)
    return jnp.sum(tiles.astype(jnp.float32), axis=0)


def taken_together(array, axis):
    everything = copy_for_each(array, axis)
    return jnp.sum(everything, axis=0)


def rms_scale(values, gain):
    inverse = lax.rsqrt(jnp.mean(values * values, axis=-1, keepdims=True) + EPS)
    return values * inverse * gain[None, :]


def per_device(stream, gain_pre, w_in, w_pool, pool_scale, w_out, gain_post):
    tok_rows = stream.shape[0]
    block_width = stream.shape[1]
    width = gain_pre.shape[1]
    group = w_pool.shape[2]
    reach = max(WINDOWS) - 1
    group_index = lax.axis_index("tp")
    window = jnp.where(
        group_index == 0, 2, jnp.where(group_index == 1, 4, jnp.where(group_index == 2, 8, 16))
    )
    positions = lax.axis_index("sp") * tok_rows + lax.iota(jnp.int32, tok_rows)
    count = jnp.minimum(positions + 1, window).astype(jnp.float32)
    gathered_in, gathered_out = rows_first((w_in, w_out), "sp", (1, 2))
    current = stream
    feature_start = group_index * block_width
    for layer in range(LAYERS):
        full_rows = gather_directly(current, "tp", 1)
        normed = rms_scale(full_rows.astype(jnp.float32), gain_pre[layer]).astype(jnp.bfloat16)
        inner_sum = jnp.dot(normed, gathered_in[layer], preferred_element_type=jnp.float32)
        inner = inner_sum.astype(jnp.bfloat16)
        rim = from_behind(inner[tok_rows - reach :], "sp", 1)
        extended = jnp.concatenate([rim, inner], axis=0).astype(jnp.float32)
        summed = jnp.zeros((tok_rows, group), jnp.float32)
        for offset in range(max(WINDOWS)):
            window_slice = extended[reach - offset : reach - offset + tok_rows]
            summed = summed + jnp.where(offset < window, window_slice, 0.0)
        pooled = summed / count[:, None]
        spread = (pooled - inner.astype(jnp.float32)).astype(jnp.bfloat16)
        mixed = jnp.dot(spread, w_pool[layer, 0], preferred_element_type=jnp.float32)
        mixed = (mixed * pool_scale[layer][None, :]).astype(jnp.bfloat16)
        partial_value = jnp.dot(mixed, gathered_out[layer], preferred_element_type=jnp.float32)
        partial_value = partial_value.astype(jnp.bfloat16)
        branch = sent_and_summed(partial_value, "tp", 1)
        squares = taken_together(jnp.sum(branch * branch, axis=1), "tp")
        inverse = lax.rsqrt(squares / width + EPS)
        gain_block = lax.dynamic_slice_in_dim(gain_post[layer], feature_start, block_width, 0)
        normed_branch = branch * inverse[:, None] * gain_block[None, :]
        current = (current.astype(jnp.float32) + normed_branch).astype(jnp.bfloat16)
    return current


def solution(mesh):
    return jax.shard_map(
        per_device,
        mesh=mesh,
        in_specs=(
            P(("grp", "sp"), "tp"),
            P(),
            P(None, "sp", "tp"),
            P(None, "tp", None, None),
            P(None, "tp"),
            P(None, "tp", "sp"),
            P(),
        ),
        out_specs=P(("grp", "sp"), "tp"),
        check_vma=False,
    )
```

profile of v0, /device:TPU:33, one launch (start us, length us, event | category | flops | bytes accessed | tf_op | source)
XLA Modules:
  0.0 364.8 jit_solution(6693995348859287650)
XLA Ops:
  6.6 1.1 copy.27
  7.6 1.7 pad_maximum_fusion
  9.4 1.2 copy.26
  10.7 1.5 broadcast_in_dim.81
  12.2 5.2 %all-to-all-start = ((bf16[4,256,1024]{1,2,0:T(8,128)(2,1)}), bf16[4,256,1024]{1,2,0:T(8,128)(2,1)S(1)}, u32[]{:S(2)}, u32[]{:S(2)}) async-start(bf16[4,256,1024]{1,2,0:T(8,128)(2,1)} %broadcast_in_dim.81), calls=%async_computation | async-start | bytes 4194304 | tf_op jit(solution)/shard_map/all_to_all | solution.py:33
  17.6 15.2 %all-to-all-done = bf16[4,256,1024]{1,2,0:T(8,128)(2,1)S(1)} async-done(((bf16[4,256,1024]{1,2,0:T(8,128)(2,1)}), bf16[4,256,1024]{1,2,0:T(8,128)(2,1)S(1)}, u32[]{:S(2)}, u32[]{:S(2)}) %all-to-all-start) | async-done | bytes 2097184 | tf_op jit(solution)/shard_map/all_to_all | solution.py:33
  32.8 0.6 fusion
  33.3 1.7 fusion.2
  35.0 101.4 %all-gather.2.cloned.1.call-done = bf16[4096,1536]{0,1:T(8,128)(2,1)} async-done(((bf16[128,1536]{0,1:T(8,128)(2,1)}), bf16[4096,1536]{0,1:T(8,128)(2,1)}) %all-gather.2.cloned.1.call-update) | async-done | bytes 12582928 | tf_op jit(solution)/shard_map/all_gather | solution.py:15
  136.4 8.4 %fusion.207 = (bf16[4096,768]{0,1:T(8,128)(2,1)S(1)}, bf16[4096,768]{0,1:T(8,128)(2,1)}) fusion(bf16[4096,1536]{0,1:T(8,128)(2,1)} %all-gather.2.cloned.1.call-done), kind=kLoop, calls=%fused_computation.233 | loop fusion | bytes 25165824 | tf_op jit(solution)/shard_map/split | solution.py:16
  144.8 2.7 copy-done
  147.5 0.8 fusion.15
  148.3 4.7 %collective-permute-start = (bf16[15,256]{1,0:T(8,128)(2,1)S(1)}, bf16[15,256]{1,0:T(8,128)(2,1)S(1)}, u32[]{:S(2)}, u32[]{:S(2)}) collective-permute-start(bf16[15,256]{1,0:T(8,128)(2,1)S(1)} %slice.277), channel_id=1, source_target_pairs={{0,4},{4,8},{8,12},{12,16},{16,20},{20,24},{24,28},{28,32},{32,36}... | collective-permute-start | bytes 23048 | tf_op jit(solution)/shard_map/ppermute | solution.py:28
  153.0 0.7 collective-permute-done
  153.8 3.0 convolution_convert_fusion.2
  156.8 1.6 copy.47
  158.4 4.1 %all-to-all-start.1 = ((bf16[4,256,1024]{2,1,0:T(8,128)(2,1)}), bf16[4,256,1024]{2,1,0:T(8,128)(2,1)S(1)}, u32[]{:S(2)}, u32[]{:S(2)}) async-start(bf16[4,256,1024]{2,1,0:T(8,128)(2,1)} %bitcast.87), calls=%async_computation.1 | async-start | bytes 4194304 | tf_op jit(solution)/shard_map/all_to_all | solution.py:54
  162.5 25.9 %all-to-all-done.1 = bf16[4,256,1024]{2,1,0:T(8,128)(2,1)S(1)} async-done(((bf16[4,256,1024]{2,1,0:T(8,128)(2,1)}), bf16[4,256,1024]{2,1,0:T(8,128)(2,1)S(1)}, u32[]{:S(2)}, u32[]{:S(2)}) %all-to-all-start.1) | async-done | bytes 2097184 | tf_op jit(solution)/shard_map/all_to_all | solution.py:54
  189.0 0.6 broadcast_in_dim.83
  189.6 3.3 all-to-all-start.2
  193.0 4.0 %all-to-all-done.2 = f32[4,1,256]{2,1,0:T(1,128)S(1)} async-done(((f32[4,1,256]{2,1,0:T(1,128)}), f32[4,1,256]{2,1,0:T(1,128)S(1)}, u32[]{:S(2)}, u32[]{:S(2)}) %all-to-all-start.2) | async-done | bytes 4128 | tf_op jit(solution)/shard_map/all_to_all | solution.py:33
  197.0 1.3 add_convert_fusion.2
  198.5 1.5 broadcast_in_dim.84
  200.0 3.7 %all-to-all-start.3 = ((bf16[4,256,1024]{1,2,0:T(8,128)(2,1)}), bf16[4,256,1024]{1,2,0:T(8,128)(2,1)S(1)}, u32[]{:S(2)}, u32[]{:S(2)}) async-start(bf16[4,256,1024]{1,2,0:T(8,128)(2,1)} %broadcast_in_dim.84), calls=%async_computation.3 | async-start | bytes 4194304 | tf_op jit(solution)/shard_map/all_to_all | solution.py:33
  203.7 23.8 %all-to-all-done.3 = bf16[4,256,1024]{1,2,0:T(8,128)(2,1)S(1)} async-done(((bf16[4,256,1024]{1,2,0:T(8,128)(2,1)}), bf16[4,256,1024]{1,2,0:T(8,128)(2,1)S(1)}, u32[]{:S(2)}, u32[]{:S(2)}) %all-to-all-start.3) | async-done | bytes 2097184 | tf_op jit(solution)/shard_map/all_to_all | solution.py:33
  227.6 0.6 fusion.3
  228.1 0.7 fusion.5
  228.9 2.4 fusion.16
  231.3 3.0 collective-permute-start.1
  234.3 2.3 collective-permute-done.1
  236.6 3.0 convolution_convert_fusion.1
  239.8 28.6 %all_to_all.48 = bf16[4,256,1024]{2,1,0:T(8,128)(2,1)S(1)} all-to-all(bf16[4,256,1024]{2,1,0:T(8,128)(2,1)S(1)} %bitcast.88), channel_id=1, replica_groups=mesh['grp'=2,'sp'=32,'tp'=4] {'tp'}, dimensions={0} | all-to-all | bytes 4194304 | tf_op jit(solution)/shard_map/all_to_all | solution.py:54
  268.9 0.6 broadcast_in_dim.85
  269.5 3.3 all-to-all-start.5
  272.9 4.0 %all-to-all-done.5 = f32[4,1,256]{2,1,0:T(1,128)S(1)} async-done(((f32[4,1,256]{2,1,0:T(1,128)}), f32[4,1,256]{2,1,0:T(1,128)S(1)}, u32[]{:S(2)}, u32[]{:S(2)}) %all-to-all-start.5) | async-done | bytes 4128 | tf_op jit(solution)/shard_map/all_to_all | solution.py:33
  277.4 1.5 broadcast_in_dim.86
  278.9 3.9 %all-to-all-start.6 = ((bf16[4,256,1024]{1,2,0:T(8,128)(2,1)}), bf16[4,256,1024]{1,2,0:T(8,128)(2,1)S(1)}, u32[]{:S(2)}, u32[]{:S(2)}) async-start(bf16[4,256,1024]{1,2,0:T(8,128)(2,1)} %broadcast_in_dim.86), calls=%async_computation.6 | async-start | bytes 4194304 | tf_op jit(solution)/shard_map/all_to_all | solution.py:33
  282.8 23.8 %all-to-all-done.6 = bf16[4,256,1024]{1,2,0:T(8,128)(2,1)S(1)} async-done(((bf16[4,256,1024]{1,2,0:T(8,128)(2,1)}), bf16[4,256,1024]{1,2,0:T(8,128)(2,1)S(1)}, u32[]{:S(2)}, u32[]{:S(2)}) %all-to-all-start.6) | async-done | bytes 2097184 | tf_op jit(solution)/shard_map/all_to_all | solution.py:33
  307.2 0.7 fusion.8
  307.9 2.4 fusion.17
  310.3 6.9 %collective-permute-start.2 = (bf16[15,256]{1,0:T(8,128)(2,1)S(1)}, bf16[15,256]{1,0:T(8,128)(2,1)S(1)}, u32[]{:S(2)}, u32[]{:S(2)}) collective-permute-start(bf16[15,256]{1,0:T(8,128)(2,1)S(1)} %slice.315), channel_id=1, source_target_pairs={{0,4},{4,8},{8,12},{12,16},{16,20},{20,24},{24,28},{28,32},{32,36}... | collective-permute-start | bytes 23048 | tf_op jit(solution)/shard_map/ppermute | solution.py:28
  317.2 0.8 collective-permute-done.2
  318.0 3.0 convolution_convert_fusion
  321.2 27.2 %all_to_all.49 = bf16[4,256,1024]{2,1,0:T(8,128)(2,1)S(1)} all-to-all(bf16[4,256,1024]{2,1,0:T(8,128)(2,1)S(1)} %bitcast.89), channel_id=1, replica_groups=mesh['grp'=2,'sp'=32,'tp'=4] {'tp'}, dimensions={0} | all-to-all | bytes 4194304 | tf_op jit(solution)/shard_map/all_to_all | solution.py:54
  348.9 0.6 broadcast_in_dim.87
  349.5 3.3 all-to-all-start.8
  352.9 4.0 %all-to-all-done.8 = f32[4,1,256]{2,1,0:T(1,128)S(1)} async-done(((f32[4,1,256]{2,1,0:T(1,128)}), f32[4,1,256]{2,1,0:T(1,128)S(1)}, u32[]{:S(2)}, u32[]{:S(2)}) %all-to-all-start.8) | async-done | bytes 4128 | tf_op jit(solution)/shard_map/all_to_all | solution.py:33
  356.9 1.0 add_convert_fusion
  (48 shorter events, 3.7 us)
Async XLA Ops:
  6.5 129.9 %all-gather.2.cloned.1.call-start = ((), (), s32[]{:S(2)}) async-start(), calls=%async_computation.9 | async-start | bytes 12976128 | tf_op jit(solution)/shard_map/all_gather | solution.py:15
  12.2 5.3 %copy-start.2 = (f32[3,4096]{1,0:T(4,128)S(1)}, f32[3,4096]{1,0:T(4,128)}, u32[]{:S(2)}) copy-start(f32[3,4096]{1,0:T(4,128)} %param.8) | copy-start | bytes 147460
  12.2 5.4 %copy-start.4 = (f32[3,256]{1,0:T(4,128)S(1)}, f32[3,256]{1,0:T(4,128)}, u32[]{:S(2)}) copy-start(f32[3,256]{1,0:T(4,128)} %param.11) | copy-start | bytes 9220
  12.2 20.6 %all-to-all-start = ((bf16[4,256,1024]{1,2,0:T(8,128)(2,1)}), bf16[4,256,1024]{1,2,0:T(8,128)(2,1)S(1)}, u32[]{:S(2)}, u32[]{:S(2)}) async-start(bf16[4,256,1024]{1,2,0:T(8,128)(2,1)} %broadcast_in_dim.81), calls=%async_computation | async-start | bytes 4194304 | tf_op jit(solution)/shard_map/all_to_all | solution.py:33
  35.0 112.5 %copy-start.1 = (bf16[4,256,1024]{1,2,0:T(8,128)(2,1)S(1)}, bf16[4,256,1024]{1,2,0:T(8,128)(2,1)}, u32[]{:S(2)}) copy-start(bf16[4,256,1024]{1,2,0:T(8,128)(2,1)} %fusion.2) | copy-start | bytes 6291460
  144.8 2.7 copy-start
  148.3 5.4 %collective-permute-start = (bf16[15,256]{1,0:T(8,128)(2,1)S(1)}, bf16[15,256]{1,0:T(8,128)(2,1)S(1)}, u32[]{:S(2)}, u32[]{:S(2)}) collective-permute-start(bf16[15,256]{1,0:T(8,128)(2,1)S(1)} %slice.277), channel_id=1, source_target_pairs={{0,4},{4,8},{8,12},{12,16},{16,20},{20,24},{24,28},{28,32},{32,36}... | collective-permute-start | bytes 23048 | tf_op jit(solution)/shard_map/ppermute | solution.py:28
  158.4 4.1 %copy-start.3 = (f32[3,4096]{1,0:T(4,128)S(1)}, f32[3,4096]{1,0:T(4,128)}, u32[]{:S(2)}) copy-start(f32[3,4096]{1,0:T(4,128)} %param.13) | copy-start | bytes 147460
  158.4 30.1 %all-to-all-start.1 = ((bf16[4,256,1024]{2,1,0:T(8,128)(2,1)}), bf16[4,256,1024]{2,1,0:T(8,128)(2,1)S(1)}, u32[]{:S(2)}, u32[]{:S(2)}) async-start(bf16[4,256,1024]{2,1,0:T(8,128)(2,1)} %bitcast.87), calls=%async_computation.1 | async-start | bytes 4194304 | tf_op jit(solution)/shard_map/all_to_all | solution.py:54
  189.6 7.4 %all-to-all-start.2 = ((f32[4,1,256]{2,1,0:T(1,128)}), f32[4,1,256]{2,1,0:T(1,128)S(1)}, u32[]{:S(2)}, u32[]{:S(2)}) async-start(f32[4,1,256]{2,1,0:T(1,128)} %broadcast_in_dim.83), calls=%async_computation.2 | async-start | bytes 8192 | tf_op jit(solution)/shard_map/all_to_all | solution.py:33
  200.0 27.6 %all-to-all-start.3 = ((bf16[4,256,1024]{1,2,0:T(8,128)(2,1)}), bf16[4,256,1024]{1,2,0:T(8,128)(2,1)S(1)}, u32[]{:S(2)}, u32[]{:S(2)}) async-start(bf16[4,256,1024]{1,2,0:T(8,128)(2,1)} %broadcast_in_dim.84), calls=%async_computation.3 | async-start | bytes 4194304 | tf_op jit(solution)/shard_map/all_to_all | solution.py:33
  231.3 5.3 %collective-permute-start.1 = (bf16[15,256]{1,0:T(8,128)(2,1)S(1)}, bf16[15,256]{1,0:T(8,128)(2,1)S(1)}, u32[]{:S(2)}, u32[]{:S(2)}) collective-permute-start(bf16[15,256]{1,0:T(8,128)(2,1)S(1)} %slice.296), channel_id=1, source_target_pairs={{0,4},{4,8},{8,12},{12,16},{16,20},{20,24},{24,28},{28,32},{32,36}... | collective-permute-start | bytes 23048 | tf_op jit(solution)/shard_map/ppermute | solution.py:28
  269.5 7.4 %all-to-all-start.5 = ((f32[4,1,256]{2,1,0:T(1,128)}), f32[4,1,256]{2,1,0:T(1,128)S(1)}, u32[]{:S(2)}, u32[]{:S(2)}) async-start(f32[4,1,256]{2,1,0:T(1,128)} %broadcast_in_dim.85), calls=%async_computation.5 | async-start | bytes 8192 | tf_op jit(solution)/shard_map/all_to_all | solution.py:33
  278.9 27.7 %all-to-all-start.6 = ((bf16[4,256,1024]{1,2,0:T(8,128)(2,1)}), bf16[4,256,1024]{1,2,0:T(8,128)(2,1)S(1)}, u32[]{:S(2)}, u32[]{:S(2)}) async-start(bf16[4,256,1024]{1,2,0:T(8,128)(2,1)} %broadcast_in_dim.86), calls=%async_computation.6 | async-start | bytes 4194304 | tf_op jit(solution)/shard_map/all_to_all | solution.py:33
  310.3 7.7 %collective-permute-start.2 = (bf16[15,256]{1,0:T(8,128)(2,1)S(1)}, bf16[15,256]{1,0:T(8,128)(2,1)S(1)}, u32[]{:S(2)}, u32[]{:S(2)}) collective-permute-start(bf16[15,256]{1,0:T(8,128)(2,1)S(1)} %slice.315), channel_id=1, source_target_pairs={{0,4},{4,8},{8,12},{12,16},{16,20},{20,24},{24,28},{28,32},{32,36}... | collective-permute-start | bytes 23048 | tf_op jit(solution)/shard_map/ppermute | solution.py:28
  349.5 7.4 %all-to-all-start.8 = ((f32[4,1,256]{2,1,0:T(1,128)}), f32[4,1,256]{2,1,0:T(1,128)S(1)}, u32[]{:S(2)}, u32[]{:S(2)}) async-start(f32[4,1,256]{2,1,0:T(1,128)} %broadcast_in_dim.87), calls=%async_computation.8 | async-start | bytes 8192 | tf_op jit(solution)/shard_map/all_to_all | solution.py:33
Sparse Core Ops, SparseCore 0:
  9.5 126.8 all-gather.1
where the time goes:
time: 366 us; the launch traced here: 365 us
  waiting for transfers between devices  206 us (56%)
  blocking collectives  55.8 us (15%)
  starting transfers between devices  41.5 us (11%)
  local copies, waits for them, and re-layouts  22.3 us (6%)
  matrix products  14.6 us (4%)
  between operations  13.8 us (4%)
  other arithmetic  10.9 us (3%)
    all_gather x1, waiting for transfers between devices, rows_first(): result = lax.all_gather(both, axis, axis=0, tiled=True)  101 us
    all_to_all x6, waiting for transfers between devices, copy_for_each(): return lax.all_to_all(copies, axis, split_axis=0, concat_axis=0, tiled=True)  74.9 us
    all_to_all x2, blocking collectives, sent_and_summed(): tiles = lax.all_to_all(in_blocks(array, dim, size), axis, 0, 0, tiled=True)  55.8 us
    all_to_all x1, waiting for transfers between devices, sent_and_summed(): tiles = lax.all_to_all(in_blocks(array, dim, size), axis, 0, 0, tiled=True)  25.9 us
    all_to_all x6, starting transfers between devices, copy_for_each(): return lax.all_to_all(copies, axis, split_axis=0, concat_axis=0, tiled=True)  22.8 us
    ppermute x3, starting transfers between devices, from_behind(): return lax.ppermute(block, axis, route)  14.5 us
    dot_general x3, matrix products, per_device(): jnp.dot(mixed, gathered_out[layer], preferred_element_type=jnp.float32)  9.05 us
    split x1, local copies, waits for them, and re-layouts, rows_first(): jnp.split(result, [sum(widths[:k]) for k in range(1, len(widths))], axis=1)  8.43 us
  transfers between devices with their start and end apart: 11, of which 11 were waited for; matrix products, arithmetic and copies ran while one was open for 1% of the time, Pallas kernels for 0%

commit v1 on v0

--- a/solution.py
+++ b/solution.py
@@ -12,7 +12,9 @@
     turned = [jnp.moveaxis(a, dim, 0) for a, dim in zip(arrays, dims)]
     widths = [t[0].size for t in turned]
     both = jnp.concatenate([t.reshape(-1, w) for t, w in zip(turned, widths)], axis=1)
-    result = lax.all_gather(both, axis, axis=0, tiled=True)
+    result = jnp.concatenate(
+        lax.all_to_all(jnp.stack([both] * lax.axis_size(axis)), axis, 0, 0), axis=0
+    )
     tiles = jnp.split(result, [sum(widths[:k]) for k in range(1, len(widths))], axis=1)
     return tuple(
         (

time: 366 us -> 834 us (2.28); the launches traced: 365 us -> 824 us
  waiting for transfers between devices: 206 us -> 612 us
  starting transfers between devices: 41.5 us -> 121 us
  blocking collectives: 55.8 us -> 35.8 us
  between operations: 13.8 us -> 0.42 us
    all_to_all x0 -> x1, waiting for transfers between devices: none -> 535 us  [rows_first(): lax.all_to_all(jnp.stack([both] * lax.axis_size(axis)), axis, 0, 0)]
    all_gather x1 -> x0, waiting for transfers between devices: 101 us -> none  [rows_first(): result = lax.all_gather(both, axis, axis=0, tiled=True)]
    ppermute x3, starting transfers between devices: 14.5 us -> 54.5 us  [from_behind(): return lax.ppermute(block, axis, route)]
    all_to_all x0 -> x1, starting transfers between devices: none -> 36.1 us  [rows_first(): lax.all_to_all(jnp.stack([both] * lax.axis_size(axis)), axis, 0, 0)]
    all_to_all x2, blocking collectives: 55.8 us -> 35.8 us  [sent_and_summed(): tiles = lax.all_to_all(in_blocks(array, dim, size), axis, 0, 0, tiled=True)]
    all_to_all x6, waiting for transfers between devices: 74.9 us -> 59.8 us  [copy_for_each(): return lax.all_to_all(copies, axis, split_axis=0, concat_axis=0, tiled=True)]
    all_to_all x1, waiting for transfers between devices: 25.9 us -> 15.2 us  [sent_and_summed(): tiles = lax.all_to_all(in_blocks(array, dim, size), axis, 0, 0, tiled=True)]
  transfers between devices with their start and end apart: 11 -> 11, of which waited for: 11 -> 11; matrix products, arithmetic and copies ran while one was open for 1% -> 0% of each run, Pallas kernels for 0% -> 0%
where the time goes in v1:
time: 834 us; the launch traced here: 824 us
  waiting for transfers between devices  612 us (73%)
  starting transfers between devices  121 us (15%)
  blocking collectives  35.8 us (4%)
  local copies, waits for them, and re-layouts  30.6 us (4%)
  matrix products  14.5 us (2%)
  other arithmetic  9.25 us (1%)
    all_to_all x1, waiting for transfers between devices, rows_first(): lax.all_to_all(jnp.stack([both] * lax.axis_size(axis)), axis, 0, 0)  535 us
    all_to_all x6, waiting for transfers between devices, copy_for_each(): return lax.all_to_all(copies, axis, split_axis=0, concat_axis=0, tiled=True)  59.8 us
    ppermute x3, starting transfers between devices, from_behind(): return lax.ppermute(block, axis, route)  54.5 us
    all_to_all x1, starting transfers between devices, rows_first(): lax.all_to_all(jnp.stack([both] * lax.axis_size(axis)), axis, 0, 0)  36.1 us
    all_to_all x2, blocking collectives, sent_and_summed(): tiles = lax.all_to_all(in_blocks(array, dim, size), axis, 0, 0, tiled=True)  35.8 us
    all_to_all x6, starting transfers between devices, copy_for_each(): return lax.all_to_all(copies, axis, split_axis=0, concat_axis=0, tiled=True)  26.2 us
  transfers between devices with their start and end apart: 11, of which 11 were waited for; matrix products, arithmetic and copies ran while one was open for 0% of the time, Pallas kernels for 0%

profile of v1, /device:TPU:33, one launch (start us, length us, event | category | flops | bytes accessed | tf_op | source)
XLA Modules:
  0.0 823.5 jit_solution(4230152748036874111)
XLA Ops:
  0.0 1.2 copy.38
  1.2 1.5 broadcast_in_dim.81
  2.7 5.2 all-to-all-start
  8.2 15.1 %all-to-all-done = bf16[4,256,1024]{1,2,0:T(8,128)(2,1)S(1)} async-done(((bf16[4,256,1024]{1,2,0:T(8,128)(2,1)}), bf16[4,256,1024]{1,2,0:T(8,128)(2,1)S(1)}, u32[]{:S(2)}, u32[]{:S(2)}) %all-to-all-start) | async-done | bytes 2097184 | tf_op jit(solution)/shard_map/all_to_all | solution.py:35
  23.3 7.3 stack.2
  30.7 36.1 %all-to-all-start.1 = ((bf16[32,128,1536]{1,2,0:T(8,128)(2,1)}), bf16[32,128,1536]{1,2,0:T(8,128)(2,1)}, u32[]{:S(2)}, u32[]{:S(2)}) async-start(bf16[32,128,1536]{1,2,0:T(8,128)(2,1)} %stack.2), calls=%async_computation.1 | async-start | bytes 25165824 | tf_op jit(solution)/shard_map/all_to_all | solution.py:16
  67.0 0.6 fusion
  67.6 1.7 fusion.2
  69.3 535.2 %all-to-all-done.1 = bf16[32,128,1536]{1,2,0:T(8,128)(2,1)} async-done(((bf16[32,128,1536]{1,2,0:T(8,128)(2,1)}), bf16[32,128,1536]{1,2,0:T(8,128)(2,1)}, u32[]{:S(2)}, u32[]{:S(2)}) %all-to-all-start.1) | async-done | bytes 12582944 | tf_op jit(solution)/shard_map/all_to_all | solution.py:16
  604.5 6.7 copy_bitcast_fusion
  611.2 3.7 fusion.207
  614.9 2.7 copy-done
  617.6 0.8 fusion.15
  618.4 15.1 %collective-permute-start = (bf16[15,256]{1,0:T(8,128)(2,1)S(1)}, bf16[15,256]{1,0:T(8,128)(2,1)S(1)}, u32[]{:S(2)}, u32[]{:S(2)}) collective-permute-start(bf16[15,256]{1,0:T(8,128)(2,1)S(1)} %slice.277), channel_id=1, source_target_pairs={{0,4},{4,8},{8,12},{12,16},{16,20},{20,24},{24,28},{28,32},{32,36}... | collective-permute-start | bytes 23048 | tf_op jit(solution)/shard_map/ppermute | solution.py:30
  633.5 0.7 collective-permute-done
  634.2 3.0 convolution_convert_fusion.2
  637.3 1.6 copy.65
  638.8 3.8 all-to-all-start.2
  642.7 15.2 %all-to-all-done.2 = bf16[4,256,1024]{2,1,0:T(8,128)(2,1)S(1)} async-done(((bf16[4,256,1024]{2,1,0:T(8,128)(2,1)}), bf16[4,256,1024]{2,1,0:T(8,128)(2,1)S(1)}, u32[]{:S(2)}, u32[]{:S(2)}) %all-to-all-start.2) | async-done | bytes 2097184 | tf_op jit(solution)/shard_map/all_to_all | solution.py:56
  658.5 0.6 broadcast_in_dim.83
  659.1 3.3 all-to-all-start.3
  662.5 4.0 all-to-all-done.3
  666.5 1.3 add_convert_fusion.2
  668.0 1.5 broadcast_in_dim.84
  669.5 3.7 all-to-all-start.4
  673.2 17.2 %all-to-all-done.4 = bf16[4,256,1024]{1,2,0:T(8,128)(2,1)S(1)} async-done(((bf16[4,256,1024]{1,2,0:T(8,128)(2,1)}), bf16[4,256,1024]{1,2,0:T(8,128)(2,1)S(1)}, u32[]{:S(2)}, u32[]{:S(2)}) %all-to-all-start.4) | async-done | bytes 2097184 | tf_op jit(solution)/shard_map/all_to_all | solution.py:35
  691.0 0.7 fusion.5
  691.7 2.4 fusion.16
  694.1 20.6 %collective-permute-start.1 = (bf16[15,256]{1,0:T(8,128)(2,1)S(1)}, bf16[15,256]{1,0:T(8,128)(2,1)S(1)}, u32[]{:S(2)}, u32[]{:S(2)}) collective-permute-start(bf16[15,256]{1,0:T(8,128)(2,1)S(1)} %slice.296), channel_id=1, source_target_pairs={{0,4},{4,8},{8,12},{12,16},{16,20},{20,24},{24,28},{28,32},{32,36}... | collective-permute-start | bytes 23048 | tf_op jit(solution)/shard_map/ppermute | solution.py:30
  714.8 0.6 collective-permute-done.1
  715.4 3.0 convolution_convert_fusion.1
  718.6 17.9 %all_to_all.53 = bf16[4,256,1024]{2,1,0:T(8,128)(2,1)S(1)} all-to-all(bf16[4,256,1024]{2,1,0:T(8,128)(2,1)S(1)} %bitcast.96), channel_id=1, replica_groups=mesh['grp'=2,'sp'=32,'tp'=4] {'tp'}, dimensions={0} | all-to-all | bytes 4194304 | tf_op jit(solution)/shard_map/all_to_all | solution.py:56
  737.0 0.6 broadcast_in_dim.85
  737.6 3.3 all-to-all-start.6
  741.0 4.1 all-to-all-done.6
  745.5 1.5 broadcast_in_dim.86
  747.0 7.2 all-to-all-start.7
  754.2 15.3 %all-to-all-done.7 = bf16[4,256,1024]{1,2,0:T(8,128)(2,1)S(1)} async-done(((bf16[4,256,1024]{1,2,0:T(8,128)(2,1)}), bf16[4,256,1024]{1,2,0:T(8,128)(2,1)S(1)}, u32[]{:S(2)}, u32[]{:S(2)}) %all-to-all-start.7) | async-done | bytes 2097184 | tf_op jit(solution)/shard_map/all_to_all | solution.py:35
  770.1 0.7 fusion.8
  770.9 2.4 fusion.17
  773.3 18.8 %collective-permute-start.2 = (bf16[15,256]{1,0:T(8,128)(2,1)S(1)}, bf16[15,256]{1,0:T(8,128)(2,1)S(1)}, u32[]{:S(2)}, u32[]{:S(2)}) collective-permute-start(bf16[15,256]{1,0:T(8,128)(2,1)S(1)} %slice.315), channel_id=1, source_target_pairs={{0,4},{4,8},{8,12},{12,16},{16,20},{20,24},{24,28},{28,32},{32,36}... | collective-permute-start | bytes 23048 | tf_op jit(solution)/shard_map/ppermute | solution.py:30
  792.1 0.8 collective-permute-done.2
  792.9 3.0 convolution_convert_fusion
  796.1 17.9 %all_to_all.54 = bf16[4,256,1024]{2,1,0:T(8,128)(2,1)S(1)} all-to-all(bf16[4,256,1024]{2,1,0:T(8,128)(2,1)S(1)} %bitcast.97), channel_id=1, replica_groups=mesh['grp'=2,'sp'=32,'tp'=4] {'tp'}, dimensions={0} | all-to-all | bytes 4194304 | tf_op jit(solution)/shard_map/all_to_all | solution.py:56
  814.5 0.6 broadcast_in_dim.87
  815.1 3.3 all-to-all-start.9
  818.4 4.0 all-to-all-done.9
  822.5 1.0 add_convert_fusion
  (53 shorter events, 4.4 us)
Async XLA Ops:
  2.7 5.3 copy-start.2
  2.7 5.4 copy-start.3
  2.7 20.6 %all-to-all-start = ((bf16[4,256,1024]{1,2,0:T(8,128)(2,1)}), bf16[4,256,1024]{1,2,0:T(8,128)(2,1)S(1)}, u32[]{:S(2)}, u32[]{:S(2)}) async-start(bf16[4,256,1024]{1,2,0:T(8,128)(2,1)} %broadcast_in_dim.81), calls=%async_computation | async-start | bytes 4194304 | tf_op jit(solution)/shard_map/all_to_all | solution.py:35
  30.7 36.1 %copy-start.4 = (f32[3,4096]{1,0:T(4,128)S(1)}, f32[3,4096]{1,0:T(4,128)}, u32[]{:S(2)}) copy-start(f32[3,4096]{1,0:T(4,128)} %param.8) | copy-start | bytes 147460
  30.7 36.3 %copy-start.6 = (f32[3,256]{1,0:T(4,128)S(1)}, f32[3,256]{1,0:T(4,128)}, u32[]{:S(2)}) copy-start(f32[3,256]{1,0:T(4,128)} %param.11) | copy-start | bytes 9220
  30.7 573.9 %all-to-all-start.1 = ((bf16[32,128,1536]{1,2,0:T(8,128)(2,1)}), bf16[32,128,1536]{1,2,0:T(8,128)(2,1)}, u32[]{:S(2)}, u32[]{:S(2)}) async-start(bf16[32,128,1536]{1,2,0:T(8,128)(2,1)} %stack.2), calls=%async_computation.1 | async-start | bytes 25165824 | tf_op jit(solution)/shard_map/all_to_all | solution.py:16
  611.2 6.4 copy-start.1
  614.9 2.7 copy-start
  618.4 15.8 %collective-permute-start = (bf16[15,256]{1,0:T(8,128)(2,1)S(1)}, bf16[15,256]{1,0:T(8,128)(2,1)S(1)}, u32[]{:S(2)}, u32[]{:S(2)}) collective-permute-start(bf16[15,256]{1,0:T(8,128)(2,1)S(1)} %slice.277), channel_id=1, source_target_pairs={{0,4},{4,8},{8,12},{12,16},{16,20},{20,24},{24,28},{28,32},{32,36}... | collective-permute-start | bytes 23048 | tf_op jit(solution)/shard_map/ppermute | solution.py:30
  638.8 3.8 copy-start.5
  638.8 19.1 %all-to-all-start.2 = ((bf16[4,256,1024]{2,1,0:T(8,128)(2,1)}), bf16[4,256,1024]{2,1,0:T(8,128)(2,1)S(1)}, u32[]{:S(2)}, u32[]{:S(2)}) async-start(bf16[4,256,1024]{2,1,0:T(8,128)(2,1)} %bitcast.95), calls=%async_computation.2 | async-start | bytes 4194304 | tf_op jit(solution)/shard_map/all_to_all | solution.py:56
  659.1 7.4 all-to-all-start.3
  669.5 20.9 %all-to-all-start.4 = ((bf16[4,256,1024]{1,2,0:T(8,128)(2,1)}), bf16[4,256,1024]{1,2,0:T(8,128)(2,1)S(1)}, u32[]{:S(2)}, u32[]{:S(2)}) async-start(bf16[4,256,1024]{1,2,0:T(8,128)(2,1)} %broadcast_in_dim.84), calls=%async_computation.4 | async-start | bytes 4194304 | tf_op jit(solution)/shard_map/all_to_all | solution.py:35
  694.1 21.2 %collective-permute-start.1 = (bf16[15,256]{1,0:T(8,128)(2,1)S(1)}, bf16[15,256]{1,0:T(8,128)(2,1)S(1)}, u32[]{:S(2)}, u32[]{:S(2)}) collective-permute-start(bf16[15,256]{1,0:T(8,128)(2,1)S(1)} %slice.296), channel_id=1, source_target_pairs={{0,4},{4,8},{8,12},{12,16},{16,20},{20,24},{24,28},{28,32},{32,36}... | collective-permute-start | bytes 23048 | tf_op jit(solution)/shard_map/ppermute | solution.py:30
  737.6 7.4 all-to-all-start.6
  747.0 22.6 %all-to-all-start.7 = ((bf16[4,256,1024]{1,2,0:T(8,128)(2,1)}), bf16[4,256,1024]{1,2,0:T(8,128)(2,1)S(1)}, u32[]{:S(2)}, u32[]{:S(2)}) async-start(bf16[4,256,1024]{1,2,0:T(8,128)(2,1)} %broadcast_in_dim.86), calls=%async_computation.7 | async-start | bytes 4194304 | tf_op jit(solution)/shard_map/all_to_all | solution.py:35
  773.3 19.6 %collective-permute-start.2 = (bf16[15,256]{1,0:T(8,128)(2,1)S(1)}, bf16[15,256]{1,0:T(8,128)(2,1)S(1)}, u32[]{:S(2)}, u32[]{:S(2)}) collective-permute-start(bf16[15,256]{1,0:T(8,128)(2,1)S(1)} %slice.315), channel_id=1, source_target_pairs={{0,4},{4,8},{8,12},{12,16},{16,20},{20,24},{24,28},{28,32},{32,36}... | collective-permute-start | bytes 23048 | tf_op jit(solution)/shard_map/ppermute | solution.py:30
  815.1 7.4 all-to-all-start.9
